TPU v7x, 32 devices: a whole 2x2x4 slice. The times are simulated.
32 devices in a mesh: fs: 16 (over z, y, x), tp: 2 (over core).
Axes of the slice: x: 2, y: 2, z: 4, core: 2. Of those that a mesh axis runs over, the one named last changes fastest.
Arguments:
- tokens: bfloat16 [2048, 2048], P('fs', 'tp'), may hold values from -300 to 300
- norm_gain: float32 [2048], P('fs'), may hold values from 0.1 to 1.9
- gate_weight: float32 [16, 2048, 1024], P(None, 'fs', 'tp'), may hold values from -1.3258252 to 1.3258252
- up_weight: float32 [16, 2048, 1024], P(None, 'fs', 'tp'), may hold values from -1.3258252 to 1.3258252
- down_weight: float32 [16, 1024, 2048], P(None, 'fs', 'tp'), may hold values from -0.1875 to 0.1875
- routes: int32 [2048, 4], P('fs'), may hold values from 0 to 15, all different within a row; in each aligned block of 128 rows (0 to 127, 128 to 255, ...) at most 64 rows name the same one
- route_weights: float32 [2048, 4], P('fs'), may hold values from 0.05 to 1
Outputs:
- mixed: bfloat16 [2048, 2048], P('fs', 'tp')
- gate_ready: bfloat16 [16, 2048, 1024], P('fs', None, 'tp')
- up_ready: bfloat16 [16, 2048, 1024], P('fs', None, 'tp')
- down_ready: bfloat16 [16, 1024, 2048], P('fs', None, 'tp')
Inputs may be any that keep to these rules, and one draw needn't show every extreme that they name: `routes`: each row names 4 different experts. In each aligned block of 128 rows no expert is named more than 64 times, a bound that some block reaches.
All inputs are finite; a program needn't handle non-finite values.
Results may differ from a plain program's by a relative error of at most 0.0089.
Values may be sent and summed in bfloat16 or wider, within the bound.
No kernel may reach another device: no remote copies, remote signals or barrier semaphores. Data moves between devices by JAX's collectives and lax.ppermute only.
A program may use at most 64 MiB of HBM per device.

v0:
```python
import jax
import jax.numpy as jnp
from jax import lax
from jax.sharding import PartitionSpec as P

epsilon = 1e-05


def activate(gate_pre, up_pre):
    gated = jnp.minimum(gate_pre, 7.0)
    upper = jnp.clip(up_pre, -7.0, 7.0)
    return (upper + 1.0) * gated * jax.nn.sigmoid(1.702 * gated)


def shards(tokens, norm_gain, gate_weight, up_weight, down_weight, routes, route_weights):
    gate_send = (norm_gain[None, :, None] * gate_weight).astype(jnp.bfloat16)
    up_send = (norm_gain[None, :, None] * up_weight).astype(jnp.bfloat16)
    down_send = down_weight.astype(jnp.bfloat16)
    gate_ready, up_ready, down_ready = (
        lax.all_to_all(gate_send, "fs", split_axis=0, concat_axis=1, tiled=True),
        lax.all_to_all(up_send, "fs", split_axis=0, concat_axis=1, tiled=True),
        lax.all_to_all(down_send, "fs", split_axis=0, concat_axis=1, tiled=True),
    )
    experts = gate_weight.shape[0]
    tok_rows = tokens.shape[0]
    top_count = routes.shape[1]
    pairs = tok_rows * top_count
    capacity = 2 * pairs // experts
    chosen = routes.reshape(pairs)
    onehot = (chosen[:, None] == jnp.arange(experts, dtype=jnp.int32)[None, :]).astype(jnp.int32)
    position = jnp.sum(jnp.cumsum(onehot, axis=0) * onehot, axis=1) - 1
    slot_index = chosen * capacity + position
    token_index = jnp.arange(pairs, dtype=jnp.int32) // top_count
    values = tokens.astype(jnp.float32)
    squared = lax.psum(jnp.sum(values * values, axis=1), "tp")
    width = values.shape[1] * lax.axis_size("tp")
    normed = (values * lax.rsqrt(squared / width + epsilon)[:, None]).astype(jnp.bfloat16)
    outbound = jnp.zeros((experts * capacity, normed.shape[1]), jnp.bfloat16)
    outbound = (
        outbound.at[slot_index].set(normed[token_index]).reshape(experts, capacity, normed.shape[1])
    )
    gate_matrix = gate_ready[0]
    up_matrix = up_ready[0]
    down_matrix = down_ready[0]
    arrived = lax.all_to_all(outbound, "fs", split_axis=0, concat_axis=0, tiled=True)
    arrived = lax.all_gather(arrived, "tp", axis=2, tiled=True)
    sources = arrived.shape[0]
    items = arrived.shape[1]
    arrived_rows = arrived.reshape(sources * items, arrived.shape[2])
    gate_pre = jnp.dot(arrived_rows, gate_matrix, preferred_element_type=jnp.float32)
    up_pre = jnp.dot(arrived_rows, up_matrix, preferred_element_type=jnp.float32)
    hidden = activate(gate_pre, up_pre).astype(jnp.bfloat16)
    summed = jnp.dot(
        lax.all_gather(hidden, "tp", axis=1, tiled=True),
        down_matrix,
        preferred_element_type=jnp.float32,
    )
    results = summed.astype(jnp.bfloat16).reshape(sources, items, down_matrix.shape[1])
    returned = lax.all_to_all(results, "fs", split_axis=0, concat_axis=0, tiled=True)
    flat_back = returned.reshape(experts * capacity, returned.shape[2])
    picked = (
        flat_back[slot_index].astype(jnp.float32).reshape(tok_rows, top_count, returned.shape[2])
    )
    mixed = jnp.sum(picked * route_weights[:, :, None], axis=1).astype(jnp.bfloat16)
    return (mixed, gate_ready, up_ready, down_ready)


def solution(mesh):
    placed = (
        P("fs", "tp"),
        P("fs"),
        P(None, "fs", "tp"),
        P(None, "fs", "tp"),
        P(None, "fs", "tp"),
        P("fs", None),
        P("fs", None),
    )
    return jax.shard_map(
        shards,
        mesh=mesh,
        in_specs=placed,
        out_specs=(P("fs", "tp"), P("fs", None, "tp"), P("fs", None, "tp"), P("fs", None, "tp")),
        check_vma=False,
    )
```

profile of v0, /device:TPU:12, one launch (start us, length us, event | category | flops | bytes accessed | tf_op | source)
XLA Modules:
  0.0 313.8 jit_solution(14182321171666740326)
XLA Ops:
  7.2 0.8 copy.13
  8.0 0.1 eq.29
  8.1 0.1 eq.25
  8.2 0.7 broadcast_multiply_fusion
  8.9 1.2 reduce-window.6
  10.0 0.2 slice_reduce_fusion
  10.3 0.1 fusion.6
  10.4 0.1 copy.12
  10.5 0.1 mul.66
  10.6 1.1 fusion.3
  11.7 2.5 psum.7
  14.2 1.1 fusion.4
  15.3 7.7 %scatter_custom_fusion = bf16[1024,1024]{1,0:T(8,128)(2,1)} fusion(s32[512]{0:T(512)S(1)} %bitcast.38, bf16[128,1024]{1,0:T(8,128)(2,1)S(1)} %fusion.4, s32[1024]{0:T(1024)S(1)} %pad_clamp_fusion.1, bf16[]{:T(256)} %constant.15.clone.1), kind=kCustom, calls=%fused_computation.8 | custom fusion | bytes 2097154 | tf_op jit(solution)/shard_map/scatter | solution.py:40
  23.0 0.0 copy-start.3
  23.0 7.3 %all-to-all-start = ((bf16[16,64,1024]{2,1,0:T(8,128)(2,1)}), bf16[16,64,1024]{2,1,0:T(8,128)(2,1)}, u32[]{:S(2)}, u32[]{:S(2)}) async-start(bf16[16,64,1024]{2,1,0:T(8,128)(2,1)} %bitcast.4), calls=%async_computation | async-start | bytes 4194304 | tf_op jit(solution)/shard_map/all_to_all | solution.py:45
  30.3 0.0 copy-done.3
  30.3 6.1 %multiply_convert_fusion = (bf16[16,128,512]{2,1,0:T(8,128)(2,1)}, bf16[16,128,512]{2,1,0:T(8,128)(2,1)S(1)}) fusion(f32[16,128,512]{2,1,0:T(8,128)} %param.9, f32[128]{0:T(128)S(1)} %copy-done.3, f32[16,128,512]{2,1,0:T(8,128)} %param.10), kind=kLoop, calls=%fused_computation.3 | loop fusion | flops 4194304 | bytes 12583424 | tf_op jit(solution)/shard_map/convert_element_type | solution.py:16
  36.4 42.3 %all-to-all-done = bf16[16,64,1024]{2,1,0:T(8,128)(2,1)} async-done(((bf16[16,64,1024]{2,1,0:T(8,128)(2,1)}), bf16[16,64,1024]{2,1,0:T(8,128)(2,1)}, u32[]{:S(2)}, u32[]{:S(2)}) %all-to-all-start) | async-done | bytes 2097184 | tf_op jit(solution)/shard_map/all_to_all | solution.py:45
  78.8 52.0 %all_to_all.46 = bf16[16,128,512]{2,1,0:T(8,128)(2,1)} all-to-all(bf16[16,128,512]{2,1,0:T(8,128)(2,1)S(1)} %get-tuple-element.5), channel_id=1, replica_groups=mesh['fs'=16,'tp'=2] {'fs'}, dimensions={0} | all-to-all | bytes 4194304 | tf_op jit(solution)/shard_map/all_to_all | solution.py:21
  130.8 5.5 %all-to-all-start.2 = ((bf16[16,128,512]{2,1,0:T(8,128)(2,1)}), bf16[16,128,512]{2,1,0:T(8,128)(2,1)}, u32[]{:S(2)}, u32[]{:S(2)}) async-start(bf16[16,128,512]{2,1,0:T(8,128)(2,1)} %get-tuple-element.4), calls=%async_computation.2 | async-start | bytes 4194304 | tf_op jit(solution)/shard_map/all_to_all | solution.py:20
  136.2 0.0 all-gather.3.cloned.1.call-start
  136.3 0.7 all-gather.3.cloned.1.call-update
  137.0 3.8 %convert_element_type.42 = bf16[16,64,1024]{2,1,0:T(8,128)(2,1)} convert(f32[16,64,1024]{2,1,0:T(8,128)} %param.11) | non-fusion elementwise | flops 1048576 | bytes 6291456 | tf_op jit(solution)/shard_map/convert_element_type | solution.py:18
  140.8 0.0 copy-start
  140.8 42.9 %all-to-all-done.2 = bf16[16,128,512]{2,1,0:T(8,128)(2,1)} async-done(((bf16[16,128,512]{2,1,0:T(8,128)(2,1)}), bf16[16,128,512]{2,1,0:T(8,128)(2,1)}, u32[]{:S(2)}, u32[]{:S(2)}) %all-to-all-start.2) | async-done | bytes 2097184 | tf_op jit(solution)/shard_map/all_to_all | solution.py:20
  183.7 4.7 %all-to-all-start.3 = ((bf16[16,64,1024]{2,1,0:T(8,128)(2,1)}), bf16[16,64,1024]{2,1,0:T(8,128)(2,1)}, u32[]{:S(2)}, u32[]{:S(2)}) async-start(bf16[16,64,1024]{2,1,0:T(8,128)(2,1)} %convert_element_type.42), calls=%async_computation.3 | async-start | bytes 4194304 | tf_op jit(solution)/shard_map/all_to_all | solution.py:22
  188.4 0.2 all-gather.5.cloned.1.call-start
  188.6 0.0 all-gather.3.cloned.1.call-done
  188.7 0.0 copy-done
  188.7 0.0 copy-start.4
  188.7 4.7 %fusion.8 = f32[1024,512]{1,0:T(8,128)S(1)} fusion(bf16[1024,2048]{1,0:T(8,128)(2,1)} %bitcast.42, bf16[2048,512]{1,0:T(8,128)(2,1)S(1)} %bitcast.35), kind=kOutput, calls=%fused_computation.34 | convolution fusion | flops 2147483648 | bytes 8388608 | tf_op jit(solution)/shard_map/dot_general | solution.py:51
  193.4 0.0 copy-done.4
  193.4 5.4 %multiply_convert_fusion.2 = bf16[1024,512]{1,0:T(8,128)(2,1)} fusion(f32[1024,512]{1,0:T(8,128)S(1)} %fusion.8, bf16[1024,2048]{1,0:T(8,128)(2,1)S(1)} %bitcast.43, bf16[2048,512]{1,0:T(8,128)(2,1)} %bitcast.7), kind=kOutput, calls=%fused_computation.6 | convolution fusion | flops 2152726528 | bytes 9437184 | tf_op jit(solution)/shard_map/dot_general | solution.py:50
  198.8 0.0 all-gather.5.cloned.1.call-update
  198.8 37.4 %all-to-all-done.3 = bf16[16,64,1024]{2,1,0:T(8,128)(2,1)} async-done(((bf16[16,64,1024]{2,1,0:T(8,128)(2,1)}), bf16[16,64,1024]{2,1,0:T(8,128)(2,1)}, u32[]{:S(2)}, u32[]{:S(2)}) %all-to-all-start.3) | async-done | bytes 2097184 | tf_op jit(solution)/shard_map/all_to_all | solution.py:22
  236.2 0.0 all-gather.5.cloned.1.call-done
  236.2 5.9 %convolution_convert_fusion = bf16[1024,1024]{1,0:T(8,128)(2,1)} fusion(bf16[1024,1024]{1,0:T(8,128)(2,1)} %all-gather.5.cloned.1.call-done, bf16[1024,1024]{1,0:T(8,128)(2,1)} %bitcast.8), kind=kOutput, calls=%fused_computation.7 | convolution fusion | flops 2148532224 | bytes 6291456 | tf_op jit(solution)/shard_map/dot_general | solution.py:53
  242.1 0.0 copy-start.2
  242.1 4.8 %all-to-all-start.4 = ((bf16[16,64,1024]{2,1,0:T(8,128)(2,1)}), bf16[16,64,1024]{2,1,0:T(8,128)(2,1)S(1)}, u32[]{:S(2)}, u32[]{:S(2)}) async-start(bf16[16,64,1024]{2,1,0:T(8,128)(2,1)} %bitcast.37), calls=%async_computation.4 | async-start | bytes 4194304 | tf_op jit(solution)/shard_map/all_to_all | solution.py:59
  246.9 0.0 copy-done.2
  246.9 0.1 copy.16
  247.0 47.5 %all-to-all-done.4 = bf16[16,64,1024]{2,1,0:T(8,128)(2,1)S(1)} async-done(((bf16[16,64,1024]{2,1,0:T(8,128)(2,1)}), bf16[16,64,1024]{2,1,0:T(8,128)(2,1)S(1)}, u32[]{:S(2)}, u32[]{:S(2)}) %all-to-all-start.4) | async-done | bytes 2097184 | tf_op jit(solution)/shard_map/all_to_all | solution.py:59
  294.6 2.0 gather_fusion
  296.6 0.7 reshape.141
  297.3 2.1 multiply_reduce_fusion
  299.4 0.0 copy-start.1
  299.4 3.2 %copy.22 = bf16[1,2048,512]{2,1,0:T(8,128)(2,1)} copy(bf16[1,2048,512]{2,1,0:T(8,128)(2,1)} %bitcast.11) | data formatting | bytes 4194304
  302.6 0.0 copy-done.1
  302.6 1.3 copy.23
  303.9 3.1 copy.24
  (9 shorter events, 0.1 us)
Async XLA Ops:
  23.0 7.3 %copy-start.3 = (f32[128]{0:T(128)S(1)}, f32[128]{0:T(128)}, u32[]{:S(2)}) copy-start(f32[128]{0:T(128)} %param.8) | copy-start | bytes 1540
  23.0 55.8 %all-to-all-start = ((bf16[16,64,1024]{2,1,0:T(8,128)(2,1)}), bf16[16,64,1024]{2,1,0:T(8,128)(2,1)}, u32[]{:S(2)}, u32[]{:S(2)}) async-start(bf16[16,64,1024]{2,1,0:T(8,128)(2,1)} %bitcast.4), calls=%async_computation | async-start | bytes 4194304 | tf_op jit(solution)/shard_map/all_to_all | solution.py:45
  130.8 52.9 %all-to-all-start.2 = ((bf16[16,128,512]{2,1,0:T(8,128)(2,1)}), bf16[16,128,512]{2,1,0:T(8,128)(2,1)}, u32[]{:S(2)}, u32[]{:S(2)}) async-start(bf16[16,128,512]{2,1,0:T(8,128)(2,1)} %get-tuple-element.4), calls=%async_computation.2 | async-start | bytes 4194304 | tf_op jit(solution)/shard_map/all_to_all | solution.py:20
  136.2 52.4 %all-gather.3.cloned.1.call-start = ((), (), s32[]{:S(2)}) async-start(), calls=%async_computation.5 | async-start | bytes 6291456 | tf_op jit(solution)/shard_map/all_gather | solution.py:46
  140.8 47.9 %copy-start = (bf16[16,128,512]{2,1,0:T(8,128)(2,1)S(1)}, bf16[16,128,512]{2,1,0:T(8,128)(2,1)}, u32[]{:S(2)}) copy-start(bf16[16,128,512]{2,1,0:T(8,128)(2,1)} %all_to_all.46) | copy-start | bytes 6291460
  183.7 52.5 %all-to-all-start.3 = ((bf16[16,64,1024]{2,1,0:T(8,128)(2,1)}), bf16[16,64,1024]{2,1,0:T(8,128)(2,1)}, u32[]{:S(2)}, u32[]{:S(2)}) async-start(bf16[16,64,1024]{2,1,0:T(8,128)(2,1)} %convert_element_type.42), calls=%async_computation.3 | async-start | bytes 4194304 | tf_op jit(solution)/shard_map/all_to_all | solution.py:22
  188.4 47.8 %all-gather.5.cloned.1.call-start = ((), (), s32[]{:S(2)}) async-start(), calls=%async_computation.6 | async-start | bytes 3145728 | tf_op jit(solution)/shard_map/all_gather | solution.py:54
  188.7 4.7 %copy-start.4 = (bf16[16,64,2048]{2,1,0:T(8,128)(2,1)S(1)}, bf16[16,64,2048]{2,1,0:T(8,128)(2,1)}, u32[]{:S(2)}) copy-start(bf16[16,64,2048]{2,1,0:T(8,128)(2,1)} %all-gather.3.cloned.1.call-done) | copy-start | bytes 12582916
  242.1 4.8 %copy-start.2 = (f32[128,4]{0,1:T(4,128)S(1)}, f32[128,4]{0,1:T(4,128)}, u32[]{:S(2)}) copy-start(f32[128,4]{0,1:T(4,128)} %param.13) | copy-start | bytes 6148
  242.1 52.5 %all-to-all-start.4 = ((bf16[16,64,1024]{2,1,0:T(8,128)(2,1)}), bf16[16,64,1024]{2,1,0:T(8,128)(2,1)S(1)}, u32[]{:S(2)}, u32[]{:S(2)}) async-start(bf16[16,64,1024]{2,1,0:T(8,128)(2,1)} %bitcast.37), calls=%async_computation.4 | async-start | bytes 4194304 | tf_op jit(solution)/shard_map/all_to_all | solution.py:59
  299.4 3.2 %copy-start.1 = (bf16[16,128,512]{2,1,0:T(8,128)(2,1)S(1)}, bf16[16,128,512]{2,1,0:T(8,128)(2,1)}, u32[]{:S(2)}) copy-start(bf16[16,128,512]{2,1,0:T(8,128)(2,1)} %all_to_all.46) | copy-start | bytes 6291460
Sparse Core Ops, SparseCore 0:
  138.6 14.8 all-gather.2
  198.9 11.6 all-gather.4
where the time goes:
time: 314 us
  waiting for transfers between devices  171 us (54%)
  blocking collectives  54.4 us (17%)
  starting transfers between devices  22.6 us (7%)
  local copies, waits for them, and re-layouts  19.6 us (6%)
  other arithmetic  16.2 us (5%)
  matrix products  16 us (5%)
  between operations  14.2 us (5%)
    all_to_all x1, blocking collectives, shards(): lax.all_to_all(up_send, 'fs', split_axis=0, concat_axis=1, tiled=True)  52 us
    all_to_all x1, waiting for transfers between devices, shards(): lax.all_to_all(results, 'fs', split_axis=0, concat_axis=0, tiled=True)  47.5 us
    all_to_all x1, waiting for transfers between devices, shards(): lax.all_to_all(gate_send, 'fs', split_axis=0, concat_axis=1, tiled=True)  42.9 us
    all_to_all x1, waiting for transfers between devices, shards(): lax.all_to_all(outbound, 'fs', split_axis=0, concat_axis=0, tiled=True)  42.3 us
    all_to_all x1, waiting for transfers between devices, shards(): lax.all_to_all(down_send, 'fs', split_axis=0, concat_axis=1, tiled=True)  37.4 us
    unnamed x15, local copies, waits for them, and re-layouts  8.51 us
    scatter x1, local copies, waits for them, and re-layouts, shards(): outbound.at[slot_index].set(normed[token_index])  7.72 us
    all_to_all x1, starting transfers between devices, shards(): lax.all_to_all(outbound, 'fs', split_axis=0, concat_axis=0, tiled=True)  7.3 us
  transfers between devices with their start and end apart: 6, of which 4 were waited for; matrix products, arithmetic and copies ran while one was open for 6% of the time, Pallas kernels for 0%

commit v1 on v0

--- a/solution.py
+++ b/solution.py
@@ -4,6 +4,18 @@
 from jax.sharding import PartitionSpec as P
 
 epsilon = 1e-05
+
+
+def split_up(x, dim, devices):
+    lengths = x.shape
+    blocks = x.reshape(*lengths[:dim], devices, lengths[dim] // devices, *lengths[dim + 1 :])
+    return jnp.moveaxis(blocks, dim, 0)
+
+
+def laid_out(blocks, dim):
+    blocks = jnp.moveaxis(blocks, 0, dim)
+    dims = blocks.shape
+    return blocks.reshape(*dims[:dim], dims[dim] * dims[dim + 1], *dims[dim + 2 :])
 
 
 def activate(gate_pre, up_pre):
@@ -42,7 +54,14 @@
     gate_matrix = gate_ready[0]
     up_matrix = up_ready[0]
     down_matrix = down_ready[0]
-    arrived = lax.all_to_all(outbound, "fs", split_axis=0, concat_axis=0, tiled=True)
+    size, index = (lax.axis_size("fs"), lax.axis_index("fs"))
+    blocks = split_up(outbound, 0, size)
+    outs = [blocks[index]]
+    for step in range(1, size):
+        sent = blocks[index ^ step]
+        outs.append(lax.ppermute(sent, "fs", [(i, i ^ step) for i in range(size)]))
+    blocks = jnp.stack(outs)[index ^ jnp.arange(size)]
+    arrived = laid_out(blocks, 0)
     arrived = lax.all_gather(arrived, "tp", axis=2, tiled=True)
     sources = arrived.shape[0]
     items = arrived.shape[1]

time: 314 us -> 297 us (0.946)
  blocking collectives: 54.4 us -> 2.46 us
  starting transfers between devices: 22.6 us -> 49.7 us
  local copies, waits for them, and re-layouts: 19.6 us -> 35 us
  waiting for transfers between devices: 171 us -> 165 us
    all_to_all x1 -> x0, blocking collectives: 52 us -> none  [shards(): lax.all_to_all(up_send, 'fs', split_axis=0, concat_axis=1, tiled=True)]
    ppermute x0 -> x15, waiting for transfers between devices: none -> 43 us  [shards(): outs.append(lax.ppermute(sent, 'fs', [(i, i ^ step) for i in range(size)]))]
    all_to_all x1, waiting for transfers between devices: 42.3 us -> 0.01 us  [shards(): lax.all_to_all(up_send, 'fs', split_axis=0, concat_axis=1, tiled=True)]
    ppermute x0 -> x15, starting transfers between devices: none -> 25 us  [shards(): outs.append(lax.ppermute(sent, 'fs', [(i, i ^ step) for i in range(size)]))]
    unnamed x15 -> x31, local copies, waits for them, and re-layouts: 8.51 us -> 17.1 us
    all_to_all x1, waiting for transfers between devices: 42.9 us -> 38.2 us  [shards(): lax.all_to_all(gate_send, 'fs', split_axis=0, concat_axis=1, tiled=True)]
    gather x0 -> x1, local copies, waits for them, and re-layouts: none -> 3.59 us  [shards(): blocks = jnp.stack(outs)[index ^ jnp.arange(size)]]
  transfers between devices with their start and end apart: 6 -> 21, of which waited for: 4 -> 15; matrix products, arithmetic and copies ran while one was open for 6% -> 14% of each run, Pallas kernels for 0% -> 0%
where the time goes in v1:
time: 297 us
  waiting for transfers between devices  165 us (56%)
  starting transfers between devices  49.7 us (17%)
  local copies, waits for them, and re-layouts  35 us (12%)
  matrix products  15.9 us (5%)
  other arithmetic  14.3 us (5%)
  between operations  14.2 us (5%)
    all_to_all x1, waiting for transfers between devices, shards(): lax.all_to_all(results, 'fs', split_axis=0, concat_axis=0, tiled=True)  47.3 us
    ppermute x15, waiting for transfers between devices, shards(): outs.append(lax.ppermute(sent, 'fs', [(i, i ^ step) for i in range(size)]))  43 us
    all_to_all x1, waiting for transfers between devices, shards(): lax.all_to_all(gate_send, 'fs', split_axis=0, concat_axis=1, tiled=True)  38.2 us
    all_to_all x1, waiting for transfers between devices, shards(): lax.all_to_all(down_send, 'fs', split_axis=0, concat_axis=1, tiled=True)  36.6 us
    ppermute x15, starting transfers between devices, shards(): outs.append(lax.ppermute(sent, 'fs', [(i, i ^ step) for i in range(size)]))  25 us
    unnamed x31, local copies, waits for them, and re-layouts  17.1 us
    scatter x1, local copies, waits for them, and re-layouts, shards(): outbound.at[slot_index].set(normed[token_index])  7.72 us
    all_to_all x1, starting transfers between devices, shards(): lax.all_to_all(up_send, 'fs', split_axis=0, concat_axis=1, tiled=True)  7.3 us
  transfers between devices with their start and end apart: 21, of which 15 were waited for; matrix products, arithmetic and copies ran while one was open for 14% of the time, Pallas kernels for 0%

profile of v1, /device:TPU:12, one launch (start us, length us, event | category | flops | bytes accessed | tf_op | source)
XLA Modules:
  0.0 296.8 jit_solution(18176437071766621119)
XLA Ops:
  7.2 6.8 %multiply_convert_fusion = (bf16[16,128,512]{2,1,0:T(8,128)(2,1)}, bf16[16,128,512]{2,1,0:T(8,128)(2,1)}) fusion(f32[16,128,512]{2,1,0:T(8,128)} %param.9, f32[128]{0:T(128)} %param.8, f32[16,128,512]{2,1,0:T(8,128)} %param.10), kind=kLoop, calls=%fused_computation.4 | loop fusion | flops 4194304 | bytes 12583424 | tf_op jit(solution)/shard_map/convert_element_type | solution.py:28
  14.0 7.3 %all-to-all-start = ((bf16[16,128,512]{2,1,0:T(8,128)(2,1)}), bf16[16,128,512]{2,1,0:T(8,128)(2,1)S(1)}, u32[]{:S(2)}, u32[]{:S(2)}) async-start(bf16[16,128,512]{2,1,0:T(8,128)(2,1)} %get-tuple-element.21), calls=%async_computation | async-start | bytes 4194304 | tf_op jit(solution)/shard_map/all_to_all | solution.py:33
  21.7 1.2 reduce-window.6
  23.6 2.5 psum.7
  26.2 7.7 %scatter_custom_fusion = bf16[1024,1024]{1,0:T(8,128)(2,1)} fusion(s32[512]{0:T(512)S(1)} %bitcast.102, bf16[128,1024]{1,0:T(8,128)(2,1)S(1)} %fusion.4, s32[1024]{0:T(1024)S(1)} %pad_clamp_fusion.2, bf16[]{:T(256)} %constant.32.clone.1), kind=kCustom, calls=%fused_computation.9 | custom fusion | bytes 2097154 | tf_op jit(solution)/shard_map/scatter | solution.py:52
  33.9 2.5 dynamic-slice_bitcast_fusion
  36.4 1.5 collective-permute-start
  37.8 0.6 collective-permute-start.1
  38.4 1.5 collective-permute-start.2
  39.9 0.6 collective-permute-start.3
  40.4 2.4 collective-permute-start.4
  42.8 7.8 %collective-permute-done = bf16[1,64,1024]{2,1,0:T(8,128)(2,1)S(1)} collective-permute-done((bf16[1,64,1024]{2,1,0:T(8,128)(2,1)S(1)}, bf16[1,64,1024]{2,1,0:T(8,128)(2,1)S(1)}, u32[]{:S(2)}, u32[]{:S(2)}) %collective-permute-start) | collective-permute-done | bytes 131104 | tf_op jit(solution)/shard_map/ppermute | solution.py:62
  50.6 1.7 collective-permute-start.5
  52.3 0.7 bitcast_dynamic-update-slice_fusion.14
  53.0 2.1 collective-permute-start.6
  55.1 0.7 bitcast_dynamic-update-slice_fusion.13
  55.7 2.0 collective-permute-done.2
  57.7 0.7 bitcast_dynamic-update-slice_fusion.12
  58.4 2.1 collective-permute-done.3
  60.4 2.3 collective-permute-start.8
  62.7 0.7 bitcast_dynamic-update-slice_fusion.11
  63.4 0.6 collective-permute-done.4
  64.0 0.9 collective-permute-start.9
  64.8 0.7 bitcast_dynamic-update-slice_fusion.10
  65.5 0.6 collective-permute-done.5
  66.1 3.2 %collective-permute-start.10 = (bf16[1,64,1024]{2,1,0:T(8,128)(2,1)S(1)}, bf16[1,64,1024]{2,1,0:T(8,128)(2,1)S(1)}, u32[]{:S(2)}, u32[]{:S(2)}) collective-permute-start(bf16[1,64,1024]{2,1,0:T(8,128)(2,1)S(1)} %get-tuple-element.8), channel_id=1, source_target_pairs={{0,22},{2,20},{4,18},{6,16},{8,30},{10,28},{12,26},{14,24},{16,6},... | collective-permute-start | bytes 393224 | tf_op jit(solution)/shard_map/ppermute | solution.py:62
  69.3 0.7 bitcast_dynamic-update-slice_fusion.9
  69.9 0.5 collective-permute-done.6
  70.4 4.0 %collective-permute-start.11 = (bf16[1,64,1024]{2,1,0:T(8,128)(2,1)S(1)}, bf16[1,64,1024]{2,1,0:T(8,128)(2,1)S(1)}, u32[]{:S(2)}, u32[]{:S(2)}) collective-permute-start(bf16[1,64,1024]{2,1,0:T(8,128)(2,1)S(1)} %get-tuple-element.7), channel_id=1, source_target_pairs={{0,24},{2,26},{4,28},{6,30},{8,16},{10,18},{12,20},{14,22},{16,8},... | collective-permute-start | bytes 393224 | tf_op jit(solution)/shard_map/ppermute | solution.py:62
  74.5 0.7 bitcast_dynamic-update-slice_fusion.8
  75.1 10.6 %collective-permute-done.7 = bf16[1,64,1024]{2,1,0:T(8,128)(2,1)S(1)} collective-permute-done((bf16[1,64,1024]{2,1,0:T(8,128)(2,1)S(1)}, bf16[1,64,1024]{2,1,0:T(8,128)(2,1)S(1)}, u32[]{:S(2)}, u32[]{:S(2)}) %collective-permute-start.7) | collective-permute-done | bytes 131104 | tf_op jit(solution)/shard_map/ppermute | solution.py:62
  85.8 3.0 %collective-permute-start.12 = (bf16[1,64,1024]{2,1,0:T(8,128)(2,1)S(1)}, bf16[1,64,1024]{2,1,0:T(8,128)(2,1)S(1)}, u32[]{:S(2)}, u32[]{:S(2)}) collective-permute-start(bf16[1,64,1024]{2,1,0:T(8,128)(2,1)S(1)} %get-tuple-element.6), channel_id=1, source_target_pairs={{0,26},{2,24},{4,30},{6,28},{8,18},{10,16},{12,22},{14,20},{16,10}... | collective-permute-start | bytes 393224 | tf_op jit(solution)/shard_map/ppermute | solution.py:62
  88.8 0.7 bitcast_dynamic-update-slice_fusion.7
  89.5 0.6 collective-permute-start.13
  90.0 0.7 bitcast_dynamic-update-slice_fusion.6
  90.7 4.9 %collective-permute-done.9 = bf16[1,64,1024]{2,1,0:T(8,128)(2,1)S(1)} collective-permute-done((bf16[1,64,1024]{2,1,0:T(8,128)(2,1)S(1)}, bf16[1,64,1024]{2,1,0:T(8,128)(2,1)S(1)}, u32[]{:S(2)}, u32[]{:S(2)}) %collective-permute-start.9) | collective-permute-done | bytes 131104 | tf_op jit(solution)/shard_map/ppermute | solution.py:62
  95.6 0.8 collective-permute-start.14
  96.4 0.7 bitcast_dynamic-update-slice_fusion.5
  97.1 4.1 %collective-permute-done.10 = bf16[1,64,1024]{2,1,0:T(8,128)(2,1)S(1)} collective-permute-done((bf16[1,64,1024]{2,1,0:T(8,128)(2,1)S(1)}, bf16[1,64,1024]{2,1,0:T(8,128)(2,1)S(1)}, u32[]{:S(2)}, u32[]{:S(2)}) %collective-permute-start.10) | collective-permute-done | bytes 131104 | tf_op jit(solution)/shard_map/ppermute | solution.py:62
  101.2 0.7 bitcast_dynamic-update-slice_fusion.4
  101.9 7.6 %collective-permute-done.11 = bf16[1,64,1024]{2,1,0:T(8,128)(2,1)S(1)} collective-permute-done((bf16[1,64,1024]{2,1,0:T(8,128)(2,1)S(1)}, bf16[1,64,1024]{2,1,0:T(8,128)(2,1)S(1)}, u32[]{:S(2)}, u32[]{:S(2)}) %collective-permute-start.11) | collective-permute-done | bytes 131104 | tf_op jit(solution)/shard_map/ppermute | solution.py:62
  109.5 0.7 bitcast_dynamic-update-slice_fusion.3
  110.1 1.6 collective-permute-done.12
  111.7 0.7 bitcast_dynamic-update-slice_fusion.2
  112.4 0.7 collective-permute-done.13
  113.1 0.7 bitcast_dynamic-update-slice_fusion.1
  113.7 6.8 %all-to-all-start.1 = ((bf16[16,128,512]{2,1,0:T(8,128)(2,1)}), bf16[16,128,512]{2,1,0:T(8,128)(2,1)}, u32[]{:S(2)}, u32[]{:S(2)}) async-start(bf16[16,128,512]{2,1,0:T(8,128)(2,1)} %get-tuple-element.20), calls=%async_computation.1 | async-start | bytes 4194304 | tf_op jit(solution)/shard_map/all_to_all | solution.py:32
  120.6 0.7 bitcast_dynamic-update-slice_fusion
  121.2 3.6 %gather_fusion = bf16[16,64,1024]{2,1,0:T(8,128)(2,1)} fusion(bf16[16,64,1024]{2,1,0:T(8,128)(2,1)} %bitcast.35, s32[1024]{0:T(1024)S(1)} %pad_clamp_fusion.1), kind=kCustom, calls=%fused_computation.1 | custom fusion | bytes 4194368 | tf_op jit(solution)/shard_map/gather | solution.py:63
  124.9 3.8 %convert_element_type.42 = bf16[16,64,1024]{2,1,0:T(8,128)(2,1)} convert(f32[16,64,1024]{2,1,0:T(8,128)} %param.11) | non-fusion elementwise | flops 1048576 | bytes 6291456 | tf_op jit(solution)/shard_map/convert_element_type | solution.py:30
  128.7 38.2 %all-to-all-done.1 = bf16[16,128,512]{2,1,0:T(8,128)(2,1)} async-done(((bf16[16,128,512]{2,1,0:T(8,128)(2,1)}), bf16[16,128,512]{2,1,0:T(8,128)(2,1)}, u32[]{:S(2)}, u32[]{:S(2)}) %all-to-all-start.1) | async-done | bytes 2097184 | tf_op jit(solution)/shard_map/all_to_all | solution.py:32
  166.8 5.7 %all-to-all-start.2 = ((bf16[16,64,1024]{2,1,0:T(8,128)(2,1)}), bf16[16,64,1024]{2,1,0:T(8,128)(2,1)}, u32[]{:S(2)}, u32[]{:S(2)}) async-start(bf16[16,64,1024]{2,1,0:T(8,128)(2,1)} %convert_element_type.42), calls=%async_computation.2 | async-start | bytes 4194304 | tf_op jit(solution)/shard_map/all_to_all | solution.py:34
  172.6 4.7 %fusion.9 = f32[1024,512]{1,0:T(8,128)S(1)} fusion(bf16[1024,2048]{1,0:T(8,128)(2,1)} %bitcast.106, bf16[2048,512]{1,0:T(8,128)(2,1)S(1)} %bitcast.98), kind=kOutput, calls=%fused_computation.69 | convolution fusion | flops 2147483648 | bytes 8388608 | tf_op jit(solution)/shard_map/dot_general | solution.py:70
  177.3 5.4 %multiply_convert_fusion.2 = bf16[1024,512]{1,0:T(8,128)(2,1)} fusion(f32[1024,512]{1,0:T(8,128)S(1)} %fusion.9, bf16[1024,2048]{1,0:T(8,128)(2,1)S(1)} %bitcast.107, bf16[2048,512]{1,0:T(8,128)(2,1)} %bitcast.39), kind=kOutput, calls=%fused_computation.7 | convolution fusion | flops 2152726528 | bytes 9437184 | tf_op jit(solution)/shard_map/dot_general | solution.py:69
  182.7 36.6 %all-to-all-done.2 = bf16[16,64,1024]{2,1,0:T(8,128)(2,1)} async-done(((bf16[16,64,1024]{2,1,0:T(8,128)(2,1)}), bf16[16,64,1024]{2,1,0:T(8,128)(2,1)}, u32[]{:S(2)}, u32[]{:S(2)}) %all-to-all-start.2) | async-done | bytes 2097184 | tf_op jit(solution)/shard_map/all_to_all | solution.py:34
  219.3 5.9 %convolution_convert_fusion = bf16[1024,1024]{1,0:T(8,128)(2,1)} fusion(bf16[1024,1024]{1,0:T(8,128)(2,1)} %all-gather.4.cloned.1.call-done, bf16[1024,1024]{1,0:T(8,128)(2,1)} %bitcast.40), kind=kOutput, calls=%fused_computation.8 | convolution fusion | flops 2148532224 | bytes 6291456 | tf_op jit(solution)/shard_map/dot_general | solution.py:72
  225.2 4.9 %all-to-all-start.3 = ((bf16[16,64,1024]{2,1,0:T(8,128)(2,1)}), bf16[16,64,1024]{2,1,0:T(8,128)(2,1)S(1)}, u32[]{:S(2)}, u32[]{:S(2)}) async-start(bf16[16,64,1024]{2,1,0:T(8,128)(2,1)} %bitcast.101), calls=%async_computation.3 | async-start | bytes 4194304 | tf_op jit(solution)/shard_map/all_to_all | solution.py:78
  230.2 47.3 %all-to-all-done.3 = bf16[16,64,1024]{2,1,0:T(8,128)(2,1)S(1)} async-done(((bf16[16,64,1024]{2,1,0:T(8,128)(2,1)}), bf16[16,64,1024]{2,1,0:T(8,128)(2,1)S(1)}, u32[]{:S(2)}, u32[]{:S(2)}) %all-to-all-start.3) | async-done | bytes 2097184 | tf_op jit(solution)/shard_map/all_to_all | solution.py:78
  277.5 2.0 gather_fusion.1
  279.5 0.7 reshape.157
  280.2 2.1 multiply_reduce_fusion
  282.3 3.2 %copy.37 = bf16[1,2048,512]{2,1,0:T(8,128)(2,1)} copy(bf16[1,2048,512]{2,1,0:T(8,128)(2,1)} %bitcast.43) | data formatting | bytes 4194304
  285.5 1.3 copy.38
  286.8 3.1 %copy.39 = bf16[1,1024,1024]{2,1,0:T(8,128)(2,1)} copy(bf16[1,1024,1024]{2,1,0:T(8,128)(2,1)} %bitcast.45) | data formatting | bytes 4194304
  (45 shorter events, 1.5 us)
Async XLA Ops:
  14.0 7.3 %copy-start.3 = (s32[128,4]{0,1:T(4,128)S(1)}, s32[128,4]{0,1:T(4,128)}, u32[]{:S(2)}) copy-start(s32[128,4]{0,1:T(4,128)} %param.12) | copy-start | bytes 6148
  14.0 9.4 %copy-start.2 = (bf16[128,1024]{1,0:T(8,128)(2,1)S(1)}, bf16[128,1024]{1,0:T(8,128)(2,1)}, u32[]{:S(2)}) copy-start(bf16[128,1024]{1,0:T(8,128)(2,1)} %param.7) | copy-start | bytes 786436
  14.0 99.7 %all-to-all-start = ((bf16[16,128,512]{2,1,0:T(8,128)(2,1)}), bf16[16,128,512]{2,1,0:T(8,128)(2,1)S(1)}, u32[]{:S(2)}, u32[]{:S(2)}) async-start(bf16[16,128,512]{2,1,0:T(8,128)(2,1)} %get-tuple-element.21), calls=%async_computation | async-start | bytes 4194304 | tf_op jit(solution)/shard_map/all_to_all | solution.py:33
  36.4 14.2 %collective-permute-start = (bf16[1,64,1024]{2,1,0:T(8,128)(2,1)S(1)}, bf16[1,64,1024]{2,1,0:T(8,128)(2,1)S(1)}, u32[]{:S(2)}, u32[]{:S(2)}) collective-permute-start(bf16[1,64,1024]{2,1,0:T(8,128)(2,1)S(1)} %get-tuple-element.18), channel_id=1, source_target_pairs={{0,2},{2,0},{4,6},{6,4},{8,10},{10,8},{12,14},{14,12},{16,18},{18,... | collective-permute-start | bytes 393224 | tf_op jit(solution)/shard_map/ppermute | solution.py:62
  37.8 15.2 %collective-permute-start.1 = (bf16[1,64,1024]{2,1,0:T(8,128)(2,1)S(1)}, bf16[1,64,1024]{2,1,0:T(8,128)(2,1)S(1)}, u32[]{:S(2)}, u32[]{:S(2)}) collective-permute-start(bf16[1,64,1024]{2,1,0:T(8,128)(2,1)S(1)} %get-tuple-element.17), channel_id=1, source_target_pairs={{0,4},{2,6},{4,0},{6,2},{8,12},{10,14},{12,8},{14,10},{16,20},{18,... | collective-permute-start | bytes 393224 | tf_op jit(solution)/shard_map/ppermute | solution.py:62
  38.4 19.3 %collective-permute-start.2 = (bf16[1,64,1024]{2,1,0:T(8,128)(2,1)S(1)}, bf16[1,64,1024]{2,1,0:T(8,128)(2,1)S(1)}, u32[]{:S(2)}, u32[]{:S(2)}) collective-permute-start(bf16[1,64,1024]{2,1,0:T(8,128)(2,1)S(1)} %get-tuple-element.16), channel_id=1, source_target_pairs={{0,6},{2,4},{4,2},{6,0},{8,14},{10,12},{12,10},{14,8},{16,22},{18,... | collective-permute-start | bytes 393224 | tf_op jit(solution)/shard_map/ppermute | solution.py:62
  39.9 20.6 %collective-permute-start.3 = (bf16[1,64,1024]{2,1,0:T(8,128)(2,1)S(1)}, bf16[1,64,1024]{2,1,0:T(8,128)(2,1)S(1)}, u32[]{:S(2)}, u32[]{:S(2)}) collective-permute-start(bf16[1,64,1024]{2,1,0:T(8,128)(2,1)S(1)} %get-tuple-element.15), channel_id=1, source_target_pairs={{0,8},{2,10},{4,12},{6,14},{8,0},{10,2},{12,4},{14,6},{16,24},{18,... | collective-permute-start | bytes 393224 | tf_op jit(solution)/shard_map/ppermute | solution.py:62
  40.4 23.5 %collective-permute-start.4 = (bf16[1,64,1024]{2,1,0:T(8,128)(2,1)S(1)}, bf16[1,64,1024]{2,1,0:T(8,128)(2,1)S(1)}, u32[]{:S(2)}, u32[]{:S(2)}) collective-permute-start(bf16[1,64,1024]{2,1,0:T(8,128)(2,1)S(1)} %get-tuple-element.14), channel_id=1, source_target_pairs={{0,10},{2,8},{4,14},{6,12},{8,2},{10,0},{12,6},{14,4},{16,26},{18,... | collective-permute-start | bytes 393224 | tf_op jit(solution)/shard_map/ppermute | solution.py:62
  50.6 15.5 %collective-permute-start.5 = (bf16[1,64,1024]{2,1,0:T(8,128)(2,1)S(1)}, bf16[1,64,1024]{2,1,0:T(8,128)(2,1)S(1)}, u32[]{:S(2)}, u32[]{:S(2)}) collective-permute-start(bf16[1,64,1024]{2,1,0:T(8,128)(2,1)S(1)} %get-tuple-element.13), channel_id=1, source_target_pairs={{0,12},{2,14},{4,8},{6,10},{8,4},{10,6},{12,0},{14,2},{16,28},{18,... | collective-permute-start | bytes 393224 | tf_op jit(solution)/shard_map/ppermute | solution.py:62
  53.0 17.4 %collective-permute-start.6 = (bf16[1,64,1024]{2,1,0:T(8,128)(2,1)S(1)}, bf16[1,64,1024]{2,1,0:T(8,128)(2,1)S(1)}, u32[]{:S(2)}, u32[]{:S(2)}) collective-permute-start(bf16[1,64,1024]{2,1,0:T(8,128)(2,1)S(1)} %get-tuple-element.12), channel_id=1, source_target_pairs={{0,14},{2,12},{4,10},{6,8},{8,6},{10,4},{12,2},{14,0},{16,30},{18,... | collective-permute-start | bytes 393224 | tf_op jit(solution)/shard_map/ppermute | solution.py:62
  57.7 28.1 %collective-permute-start.7 = (bf16[1,64,1024]{2,1,0:T(8,128)(2,1)S(1)}, bf16[1,64,1024]{2,1,0:T(8,128)(2,1)S(1)}, u32[]{:S(2)}, u32[]{:S(2)}) collective-permute-start(bf16[1,64,1024]{2,1,0:T(8,128)(2,1)S(1)} %get-tuple-element.11), channel_id=1, source_target_pairs={{0,16},{2,18},{4,20},{6,22},{8,24},{10,26},{12,28},{14,30},{16,0},... | collective-permute-start | bytes 393224 | tf_op jit(solution)/shard_map/ppermute | solution.py:62
  60.4 29.0 %collective-permute-start.8 = (bf16[1,64,1024]{2,1,0:T(8,128)(2,1)S(1)}, bf16[1,64,1024]{2,1,0:T(8,128)(2,1)S(1)}, u32[]{:S(2)}, u32[]{:S(2)}) collective-permute-start(bf16[1,64,1024]{2,1,0:T(8,128)(2,1)S(1)} %get-tuple-element.10), channel_id=1, source_target_pairs={{0,18},{2,16},{4,22},{6,20},{8,26},{10,24},{12,30},{14,28},{16,2},... | collective-permute-start | bytes 393224 | tf_op jit(solution)/shard_map/ppermute | solution.py:62
  64.0 31.6 %collective-permute-start.9 = (bf16[1,64,1024]{2,1,0:T(8,128)(2,1)S(1)}, bf16[1,64,1024]{2,1,0:T(8,128)(2,1)S(1)}, u32[]{:S(2)}, u32[]{:S(2)}) collective-permute-start(bf16[1,64,1024]{2,1,0:T(8,128)(2,1)S(1)} %get-tuple-element.9), channel_id=1, source_target_pairs={{0,20},{2,22},{4,16},{6,18},{8,28},{10,30},{12,24},{14,26},{16,4},... | collective-permute-start | bytes 393224 | tf_op jit(solution)/shard_map/ppermute | solution.py:62
  66.1 35.2 %collective-permute-start.10 = (bf16[1,64,1024]{2,1,0:T(8,128)(2,1)S(1)}, bf16[1,64,1024]{2,1,0:T(8,128)(2,1)S(1)}, u32[]{:S(2)}, u32[]{:S(2)}) collective-permute-start(bf16[1,64,1024]{2,1,0:T(8,128)(2,1)S(1)} %get-tuple-element.8), channel_id=1, source_target_pairs={{0,22},{2,20},{4,18},{6,16},{8,30},{10,28},{12,26},{14,24},{16,6},... | collective-permute-start | bytes 393224 | tf_op jit(solution)/shard_map/ppermute | solution.py:62
  70.4 39.0 %collective-permute-start.11 = (bf16[1,64,1024]{2,1,0:T(8,128)(2,1)S(1)}, bf16[1,64,1024]{2,1,0:T(8,128)(2,1)S(1)}, u32[]{:S(2)}, u32[]{:S(2)}) collective-permute-start(bf16[1,64,1024]{2,1,0:T(8,128)(2,1)S(1)} %get-tuple-element.7), channel_id=1, source_target_pairs={{0,24},{2,26},{4,28},{6,30},{8,16},{10,18},{12,20},{14,22},{16,8},... | collective-permute-start | bytes 393224 | tf_op jit(solution)/shard_map/ppermute | solution.py:62
  85.8 25.9 %collective-permute-start.12 = (bf16[1,64,1024]{2,1,0:T(8,128)(2,1)S(1)}, bf16[1,64,1024]{2,1,0:T(8,128)(2,1)S(1)}, u32[]{:S(2)}, u32[]{:S(2)}) collective-permute-start(bf16[1,64,1024]{2,1,0:T(8,128)(2,1)S(1)} %get-tuple-element.6), channel_id=1, source_target_pairs={{0,26},{2,24},{4,30},{6,28},{8,18},{10,16},{12,22},{14,20},{16,10}... | collective-permute-start | bytes 393224 | tf_op jit(solution)/shard_map/ppermute | solution.py:62
  89.5 23.6 %collective-permute-start.13 = (bf16[1,64,1024]{2,1,0:T(8,128)(2,1)S(1)}, bf16[1,64,1024]{2,1,0:T(8,128)(2,1)S(1)}, u32[]{:S(2)}, u32[]{:S(2)}) collective-permute-start(bf16[1,64,1024]{2,1,0:T(8,128)(2,1)S(1)} %get-tuple-element.5), channel_id=1, source_target_pairs={{0,28},{2,30},{4,24},{6,26},{8,20},{10,22},{12,16},{14,18},{16,12}... | collective-permute-start | bytes 393224 | tf_op jit(solution)/shard_map/ppermute | solution.py:62
  95.6 25.0 %collective-permute-start.14 = (bf16[1,64,1024]{2,1,0:T(8,128)(2,1)S(1)}, bf16[1,64,1024]{2,1,0:T(8,128)(2,1)S(1)}, u32[]{:S(2)}, u32[]{:S(2)}) collective-permute-start(bf16[1,64,1024]{2,1,0:T(8,128)(2,1)S(1)} %get-tuple-element.4), channel_id=1, source_target_pairs={{0,30},{2,28},{4,26},{6,24},{8,22},{10,20},{12,18},{14,16},{16,14}... | collective-permute-start | bytes 393224 | tf_op jit(solution)/shard_map/ppermute | solution.py:62
  113.7 58.8 %copy-start = (bf16[16,128,512]{2,1,0:T(8,128)(2,1)}, bf16[16,128,512]{2,1,0:T(8,128)(2,1)S(1)}, u32[]{:S(2)}) copy-start(bf16[16,128,512]{2,1,0:T(8,128)(2,1)S(1)} %all-to-all-done) | copy-start | bytes 6291460
  113.7 53.1 %all-to-all-start.1 = ((bf16[16,128,512]{2,1,0:T(8,128)(2,1)}), bf16[16,128,512]{2,1,0:T(8,128)(2,1)}, u32[]{:S(2)}, u32[]{:S(2)}) async-start(bf16[16,128,512]{2,1,0:T(8,128)(2,1)} %get-tuple-element.20), calls=%async_computation.1 | async-start | bytes 4194304 | tf_op jit(solution)/shard_map/all_to_all | solution.py:32
  120.5 52.0 %all-gather.6.cloned.1.call-start = ((), (), s32[]{:S(2)}) async-start(), calls=%async_computation.5 | async-start | bytes 6291456 | tf_op jit(solution)/shard_map/all_gather | solution.py:65
  166.8 52.4 %all-to-all-start.2 = ((bf16[16,64,1024]{2,1,0:T(8,128)(2,1)}), bf16[16,64,1024]{2,1,0:T(8,128)(2,1)}, u32[]{:S(2)}, u32[]{:S(2)}) async-start(bf16[16,64,1024]{2,1,0:T(8,128)(2,1)} %convert_element_type.42), calls=%async_computation.2 | async-start | bytes 4194304 | tf_op jit(solution)/shard_map/all_to_all | solution.py:34
  172.5 46.8 %all-gather.4.cloned.1.call-start = ((), (), s32[]{:S(2)}) async-start(), calls=%async_computation.4 | async-start | bytes 3145728 | tf_op jit(solution)/shard_map/all_gather | solution.py:73
  172.6 4.7 %copy-start.5 = (bf16[16,64,2048]{2,1,0:T(8,128)(2,1)S(1)}, bf16[16,64,2048]{2,1,0:T(8,128)(2,1)}, u32[]{:S(2)}) copy-start(bf16[16,64,2048]{2,1,0:T(8,128)(2,1)} %all-gather.6.cloned.1.call-done) | copy-start | bytes 12582916
  225.2 4.9 %copy-start.4 = (f32[128,4]{0,1:T(4,128)S(1)}, f32[128,4]{0,1:T(4,128)}, u32[]{:S(2)}) copy-start(f32[128,4]{0,1:T(4,128)} %param.13) | copy-start | bytes 6148
  225.2 52.3 %all-to-all-start.3 = ((bf16[16,64,1024]{2,1,0:T(8,128)(2,1)}), bf16[16,64,1024]{2,1,0:T(8,128)(2,1)S(1)}, u32[]{:S(2)}, u32[]{:S(2)}) async-start(bf16[16,64,1024]{2,1,0:T(8,128)(2,1)} %bitcast.101), calls=%async_computation.3 | async-start | bytes 4194304 | tf_op jit(solution)/shard_map/all_to_all | solution.py:78
  282.3 3.2 %copy-start.1 = (bf16[16,128,512]{2,1,0:T(8,128)(2,1)S(1)}, bf16[16,128,512]{2,1,0:T(8,128)(2,1)}, u32[]{:S(2)}) copy-start(bf16[16,128,512]{2,1,0:T(8,128)(2,1)} %copy-done) | copy-start | bytes 6291460
Sparse Core Ops, SparseCore 0:
  125.0 14.7 all-gather.5
  182.8 11.7 all-gather.3
